TPU v7x, 32 devices: a whole 2x2x4 slice. The times are simulated.
32 devices in a mesh: ep: 8 (over z, x), tp: 4 (over y, core).
Axes of the slice: x: 2, y: 2, z: 4, core: 2. Of those that a mesh axis runs over, the one named last changes fastest.
Arguments:
- queries: bfloat16 [1024, 2048], P('ep', 'tp'), may hold values from -60 to 60
- keys: bfloat16 [1024, 512], P('ep', 'tp'), may hold values from -60 to 60
- values: bfloat16 [1024, 512], P('ep', 'tp'), may hold values from -6 to 6
- cum_gates: float32 [1024, 16], P('ep', 'tp'), may hold values from -259 to 0, as said below
- expert_in: bfloat16 [4096, 4096], P(('ep', 'tp')), may hold values from -6 to 6
- norm_gain: float32 [4096], replicated, may hold values from 0.1 to 1.9
- route_group: int32 [4096, 1], P(('ep', 'tp')), may hold values from 0 to 7; in each aligned block of 128 rows (0 to 127, 128 to 255, ...) at most 24 rows name the same one
- route_member: int32 [4096, 2], P(('ep', 'tp')), may hold values from 0 to 3, all different within a row
- route_weight: float32 [4096, 2], P(('ep', 'tp')), may hold values from 0.1 to 1
- w_gate: bfloat16 [32, 4096, 384], P(('ep', 'tp')), may hold values from -0.09375 to 0.09375
- w_up: bfloat16 [32, 4096, 384], P(('ep', 'tp')), may hold values from -0.09375 to 0.09375
- w_down: bfloat16 [32, 384, 4096], P(('ep', 'tp')), may hold values from -0.3125 to 0.3125
Outputs:
- attended: bfloat16 [1024, 2048], P('ep', 'tp')
- expert_out: bfloat16 [4096, 4096], P(('ep', 'tp'))
Inputs may be any that keep to these rules, and one draw needn't show every extreme that they name: `cum_gates`: each head's entries never rise along positions. `route_group`: at most 24 of the rows of one device name one group. `route_member`: the 2 entries of a row differ.
All inputs are finite; a program needn't handle non-finite values.
Results may differ from a plain program's by a relative error of at most 0.0075.
Values may be sent and summed in bfloat16 or wider, within the bound.
A program may use at most 128 MiB of HBM per device.

v0:
```python
import functools
import math

import jax
import jax.numpy as jnp
from jax import lax
from jax.experimental import pallas as pl
from jax.experimental.pallas import tpu as pltpu
from jax.sharding import PartitionSpec as P

HEAD_WIDTH = 128
GROUP = 4
TOP = 2


NEGATIVE = -1e30
EPSILON = 1e-06


def group_fold(states, prepared_group, key_piece, value_piece, start_row, all_gates, key_heads):
    query_rows, query_pos, query_gates = prepared_group
    count_queries = query_rows.shape[0]
    head_count = all_gates.shape[1]
    heads_per_group = head_count // key_heads
    piece_rows = key_piece.shape[0]
    rows_per_block = math.gcd(piece_rows, 512)
    score_scale = HEAD_WIDTH ** (-0.5)

    def key_step(step_index, carried):
        running, totals, accumulated = carried
        offset = step_index * rows_per_block
        key_rows = lax.dynamic_slice_in_dim(key_piece, offset, rows_per_block, 0).reshape(
            rows_per_block, key_heads, HEAD_WIDTH
        )
        rows_of_value = lax.dynamic_slice_in_dim(value_piece, offset, rows_per_block, 0).reshape(
            rows_per_block, key_heads, HEAD_WIDTH
        )
        key_gates = lax.dynamic_slice_in_dim(all_gates, offset, rows_per_block, 0)
        key_pos = offset + jnp.arange(rows_per_block, dtype=jnp.int32)
        scores = jnp.einsum(
            "qgrd,kgd->grqk", query_rows, key_rows, preferred_element_type=jnp.float32
        )
        scores = scores.reshape(head_count, count_queries, rows_per_block) * score_scale
        scores = scores + query_gates.T[:, :, None] - key_gates.T[:, None, :]
        allowed = (key_pos[None, :] <= query_pos[:, None])[None]
        scores = jnp.where(allowed, scores, NEGATIVE)
        new_max = jnp.maximum(running, jnp.max(scores, axis=-1))
        weights = jnp.where(allowed, jnp.exp(scores - new_max[..., None]), 0.0)
        factor = jnp.exp(running - new_max)
        totals = totals * factor + jnp.sum(weights, axis=-1)
        inner_product = jnp.einsum(
            "tjub,btl->tjul",
            weights.astype(jnp.bfloat16).reshape(
                key_heads, heads_per_group, count_queries, rows_per_block
            ),
            rows_of_value,
            preferred_element_type=jnp.float32,
        )
        accumulated = accumulated * factor[..., None] + inner_product.reshape(
            head_count, count_queries, HEAD_WIDTH
        )
        return (new_max, totals, accumulated)

    def run_all(carried):
        return lax.fori_loop(0, piece_rows // rows_per_block, key_step, carried)

    def keep_state(carried):
        return carried

    return lax.cond(start_row <= query_pos[-1], run_all, keep_state, states)


def fold_attention(groups, keys, values, all_gates):
    key_heads = keys.shape[1] // HEAD_WIDTH
    head_count = all_gates.shape[1]
    prepared = []
    initial = []
    for query_block, query_pos in groups:
        count_queries = query_block.shape[0]
        prepared.append(
            (
                query_block.reshape(count_queries, key_heads, head_count // key_heads, HEAD_WIDTH),
                query_pos,
                all_gates[query_pos],
            )
        )
        initial.append(
            (
                jnp.full((head_count, count_queries), NEGATIVE, jnp.float32),
                jnp.zeros((head_count, count_queries), jnp.float32),
                jnp.zeros((head_count, count_queries, HEAD_WIDTH), jnp.float32),
            )
        )
    carried = tuple(initial)
    start_row = jnp.int32(0)
    key_piece = lax.all_gather(keys, "ep", axis=0, tiled=True)
    value_piece = lax.all_gather(values, "ep", axis=0, tiled=True)
    finals = tuple(
        (
            group_fold(
                states, prepared_group, key_piece, value_piece, start_row, all_gates, key_heads
            )
            for states, prepared_group in zip(carried, prepared)
        )
    )
    outputs = []
    for running, totals, accumulated in finals:
        result = accumulated / totals[..., None]
        outputs.append(
            jnp.transpose(result, (1, 0, 2))
            .reshape(result.shape[1], head_count * HEAD_WIDTH)
            .astype(jnp.bfloat16)
        )
    return outputs


def attention_half(queries, keys, values, cum_gates):
    count_rows = queries.shape[0]
    head_count = cum_gates.shape[1]
    ep_index = lax.axis_index("ep")
    all_gates = lax.all_gather(cum_gates, "ep", axis=0, tiled=True)
    query_heads = queries.reshape(count_rows, head_count, HEAD_WIDTH)
    positions = ep_index * count_rows + jnp.arange(count_rows, dtype=jnp.int32)
    outputs = fold_attention([(query_heads, positions)], keys, values, all_gates)
    attended = outputs[0]
    return attended


def expert_half(
    expert_in, norm_gain, route_group, route_member, route_weight, w_gate, w_up, w_down
):
    count_rows, model_width = expert_in.shape
    ep_size = lax.axis_size("ep")
    tp_size = lax.axis_size("tp")
    capacity = max(2, (3 * count_rows + 2 * ep_size - 1) // (2 * ep_size))
    floats = expert_in.astype(jnp.float32)
    normed = (
        floats * lax.rsqrt(jnp.mean(floats * floats, axis=-1, keepdims=True) + EPSILON) * norm_gain
    ).astype(jnp.bfloat16)
    members = jnp.arange(GROUP, dtype=jnp.int32)
    mix_weights = jnp.zeros((count_rows, GROUP), jnp.float32)
    for rank_index in range(TOP):
        mix_weights = mix_weights + route_weight[:, rank_index : rank_index + 1] * (
            route_member[:, rank_index : rank_index + 1] == members[None, :]
        ).astype(jnp.float32)
    mix_weights = mix_weights.astype(jnp.bfloat16)
    group_ids = route_group[:, 0]
    group_match = (group_ids[:, None] == jnp.arange(ep_size, dtype=jnp.int32)[None, :]).astype(
        jnp.int32
    )
    rank_within = jnp.sum((jnp.cumsum(group_match, axis=0) - group_match) * group_match, axis=1)
    slot_of_row = group_ids * capacity + rank_within
    row_of_slot = (
        jnp.full((ep_size * capacity,), count_rows, jnp.int32)
        .at[slot_of_row]
        .set(jnp.arange(count_rows, dtype=jnp.int32))
    )
    padded_rows = jnp.concatenate([normed, jnp.zeros((1, model_width), jnp.bfloat16)], axis=0)
    padded_weights = jnp.concatenate([mix_weights, jnp.zeros((1, GROUP), jnp.bfloat16)], axis=0)
    send_rows = padded_rows[row_of_slot].reshape(ep_size, capacity, model_width)
    send_weights = padded_weights[row_of_slot].reshape(ep_size, capacity, GROUP)
    gate_matrix = w_gate[0]
    up_matrix = w_up[0]
    down_matrix = w_down[0]
    arrived_rows = lax.all_to_all(send_rows, "ep", split_axis=0, concat_axis=0, tiled=True)
    arrived_weights = lax.all_to_all(send_weights, "ep", split_axis=0, concat_axis=0, tiled=True)
    sources = arrived_rows.shape[0]
    per_source = arrived_rows.shape[1]
    flat_rows = arrived_rows.reshape(sources * per_source, model_width)
    pieces = lax.all_gather(flat_rows, "tp", axis=0, tiled=True)
    gate_part = jnp.dot(pieces, gate_matrix, preferred_element_type=jnp.float32)
    up_part = jnp.dot(pieces, up_matrix, preferred_element_type=jnp.float32)
    hidden = (jax.nn.silu(gate_part) * up_part).astype(jnp.bfloat16)
    expert_outputs = jnp.dot(hidden, down_matrix, preferred_element_type=jnp.float32).astype(
        jnp.bfloat16
    )
    member_outputs = lax.all_to_all(
        expert_outputs.reshape(tp_size, sources * per_source, model_width),
        "tp",
        split_axis=0,
        concat_axis=0,
        tiled=True,
    )
    flat_weights = arrived_weights.reshape(sources * per_source, GROUP).astype(jnp.float32)
    combined = jnp.zeros((sources * per_source, model_width), jnp.float32)
    for member in range(GROUP):
        combined = combined + flat_weights[:, member : member + 1] * member_outputs[member]
    mixed = combined.astype(jnp.bfloat16).reshape(sources, per_source, model_width)
    returned = lax.all_to_all(mixed, "ep", split_axis=0, concat_axis=0, tiled=True)
    return returned.reshape(ep_size * capacity, model_width)[slot_of_row]


def flipped(index, bits):
    result = index
    place = 1
    while place <= bits:
        if bits & place:
            result = result + place - 2 * place * ((index // place) % 2)
        place = place * 2
    return result


def fused_kernel(
    n,
    capacity,
    queries_in,
    keys_in,
    values_in,
    gates_in,
    expert_rows,
    gain_in,
    route_group_in,
    route_member_in,
    route_weight_in,
    w_gate,
    w_up,
    w_down,
    attended_out,
    expert_result,
    queries,
    keys,
    values,
    gates,
    expert_in,
    gain,
    route_group,
    route_member,
    route_weight,
    attended,
    expert_out,
    input_sem,
    output_sem,
    send,
    pieces,
    gate_up,
    down,
    partial,
    from_core,
    to_chip,
    from_chip,
    final,
    returned,
    all_keys,
    all_values,
    own_gates,
    all_gates,
    weight_sem,
    disp_send,
    disp_recv,
    fwd_send,
    fwd_recv,
    part_send,
    part_recv,
    ret_send,
    ret_recv,
    key_send,
    key_recv,
):
    f32, bf16 = jnp.float32, jnp.bfloat16
    rows, width = expert_in.shape
    hidden_width = down.shape[0]
    wide = pieces.shape[-1]
    chunks = n // 2
    me = lax.axis_index("ep")
    mine = lax.axis_index("tp")
    core = mine % 2
    side = mine // 2
    twin = flipped(mine, 1)
    across = flipped(mine, 2)
    diagonal = flipped(mine, 3)

    inputs = (
        (route_group_in, route_group),
        (route_member_in, route_member),
        (route_weight_in, route_weight),
        (expert_rows, expert_in),
        (gain_in, gain),
        (keys_in, keys),
        (values_in, values),
        (gates_in, gates),
        (queries_in, queries),
    )
    input_copies = [
        pltpu.make_async_copy(source, target, input_sem.at[index])
        for index, (source, target) in enumerate(inputs)
    ]
    weight_copies = [
        pltpu.make_async_copy(w_gate.at[0], gate_up.at[:, pl.ds(0, hidden_width)], weight_sem.at[0]),
        pltpu.make_async_copy(
            w_up.at[0], gate_up.at[:, pl.ds(hidden_width, hidden_width)], weight_sem.at[1]
        ),
        pltpu.make_async_copy(w_down.at[0], down, weight_sem.at[2]),
    ]
    for copy in input_copies:
        copy.start()

    def has(index, bit):
        return (index // bit) % 2 == 1

    barrier = pltpu.get_barrier_semaphore()

    def remote(source, target, send_sem, recv_sem, ep, tp):
        return pltpu.make_async_remote_copy(
            src_ref=source,
            dst_ref=target,
            send_sem=send_sem,
            recv_sem=recv_sem,
            device_id={"ep": ep, "tp": tp},
            device_id_type=pl.DeviceIdType.MESH,
        )

    for step in range(1, n):
        pl.semaphore_signal(
            barrier,
            inc=1,
            device_id={"ep": flipped(me, step), "tp": mine},
            device_id_type=pl.DeviceIdType.MESH,
        )
    for other in (twin, across):
        pl.semaphore_signal(
            barrier,
            inc=1,
            device_id={"ep": me, "tp": other},
            device_id_type=pl.DeviceIdType.MESH,
        )

    for copy in weight_copies:
        copy.start()
    for copy in input_copies[:3]:
        copy.wait()

    lanes = lax.broadcasted_iota(jnp.int32, (rows, 128), 1)
    row_i = lax.broadcasted_iota(jnp.int32, (rows, rows), 0)
    col_i = lax.broadcasted_iota(jnp.int32, (rows, rows), 1)
    earlier = (col_i < row_i).astype(bf16)
    same = row_i == col_i

    def column(row):
        return jnp.sum(jnp.where(same, row.astype(f32), 0.0), axis=1, keepdims=True)

    group = column(route_group[...])
    match = (group == lanes.astype(f32)).astype(f32)
    ranks = jnp.dot(earlier, match.astype(bf16), preferred_element_type=f32)
    rank_within = jnp.sum(ranks * match, axis=1, keepdims=True)
    slot = group * float(capacity) + rank_within
    slot_row = jnp.sum(jnp.where(same, slot, 0.0), axis=0, keepdims=True)
    slots = n * capacity
    place = (
        lax.broadcasted_iota(jnp.int32, (slots, rows), 0).astype(f32) == slot_row
    ).astype(f32).astype(bf16)
    mix = jnp.zeros((rows, 128), f32)
    for rank_index in range(TOP):
        mix = mix + jnp.where(
            column(route_member[rank_index : rank_index + 1, :]) == lanes.astype(f32),
            column(route_weight[rank_index : rank_index + 1, :]),
            0.0,
        )
    for copy in input_copies[3:5]:
        copy.wait()
    floats = expert_in[...].astype(f32)
    scale = lax.rsqrt(jnp.mean(floats * floats, axis=-1, keepdims=True) + EPSILON)
    normed = (floats * scale * gain[...]).astype(bf16)
    send[:, :, pl.ds(0, width)] = (
        jnp.dot(place, normed, preferred_element_type=f32)
        .astype(bf16)
        .reshape(n, capacity, width)
    )
    send[:, :, pl.ds(width, wide - width)] = (
        jnp.dot(place, mix.astype(bf16), preferred_element_type=f32)
        .astype(bf16)
        .reshape(n, capacity, wide - width)
    )
    for copy in input_copies[5:]:
        copy.wait()
    heads = gates.shape[0]
    own_gates[pl.ds(0, heads), :] = gates[...]
    for flip in range(1, n):

        @pl.when(jnp.logical_not(has(me, 1 << (flip.bit_length() - 1))))
        def _():
            block = flipped(me, flip)
            all_keys[block] = jnp.zeros_like(all_keys[block])
            all_values[block] = jnp.zeros_like(all_values[block])
            all_gates[block] = jnp.zeros_like(all_gates[block])

    all_gates[me] = own_gates[...]
    all_keys[me] = keys[...]
    all_values[me] = values[...]

    pl.semaphore_wait(barrier, n + 1)

    def dispatch(peer):
        return remote(
            send.at[peer], pieces.at[mine, me], disp_send.at[peer], disp_recv.at[me], peer, mine
        )

    def arrival(peer):
        return remote(
            send.at[peer], pieces.at[mine, peer], disp_send.at[peer], disp_recv.at[peer], peer, mine
        )

    for step in range(1, n):
        dispatch(flipped(me, step)).start()
    pieces[mine, me] = send[me]

    shared = (all_keys, all_values, all_gates)

    bits = [1 << power for power in reversed(range((n - 1).bit_length()))]

    def high(number):
        return 1 << (number.bit_length() - 1)

    def key_send_copy(which, bit, others):
        block = shared[which].at[flipped(me, others)]
        flip = others | bit
        return remote(
            block,
            block,
            key_send.at[which, flip],
            key_recv.at[which, flip],
            flipped(me, bit),
            mine,
        )

    def key_arrival(which, flip):
        block = shared[which].at[flipped(me, flip)]
        return remote(
            block, block, key_send.at[which, flip], key_recv.at[which, flip], me, mine
        )

    def key_flips(bit):
        return [others for others in range(0, n, 2 * bit)]

    def sends_keys(bit, others):
        return has(me, high(others)) if others else jnp.logical_not(has(me, bit))

    def wait_keys(bit):
        for others in key_flips(bit):
            flip = others | bit

            @pl.when(has(me, high(flip)))
            def _():
                for which in range(3):
                    key_arrival(which, flip).wait_recv()

    def start_keys(bit):
        for others in key_flips(bit):

            @pl.when(sends_keys(bit, others))
            def _():
                for which in range(3):
                    key_send_copy(which, bit, others).start()

    def pair_of(chunk):
        return pl.ds(flipped(me // 2, chunk) * 2, 2)

    def forward(step, which):
        part = pieces.at[across if which == 2 else mine, flipped(me, step)]
        return remote(
            part,
            part,
            fwd_send.at[which, step],
            fwd_recv.at[which, step],
            me,
            across if which == 1 else twin,
        )

    def forwarded(step, which):
        part = pieces.at[(twin, across, diagonal)[which], flipped(me, step)]
        return remote(part, part, fwd_send.at[which, step], fwd_recv.at[which, step], me, twin)

    def stage_arrive(step):
        if step:
            arrival(flipped(me, step)).wait_recv()
        forward(step, 1).start()
        forward(step, 0).start()

    def stage_cross(step):
        forwarded(step, 1).wait_recv()
        forward(step, 2).start()

    def core_copy(chunk):
        pair = pair_of(chunk)
        return remote(
            partial.at[:, 1 - core, pair],
            from_core.at[:, pair],
            part_send.at[0, chunk],
            part_recv.at[0, chunk],
            me,
            twin,
        )

    def chip_copy(step):
        source = flipped(me, step)
        return remote(
            to_chip.at[source],
            from_chip.at[source],
            part_send.at[1, step],
            part_recv.at[1, step],
            me,
            across,
        )

    def stage_compute(chunk):
        for step in (chunk * 2, chunk * 2 + 1):
            forwarded(step, 0).wait_recv()
            forwarded(step, 2).wait_recv()
        pair = pair_of(chunk)
        count = 4 * 2 * capacity
        held = pieces[:, pair, :, pl.ds(0, width)].reshape(count, width)
        both = jnp.dot(held, gate_up[...], preferred_element_type=f32)
        gate_part = both[:, :hidden_width]
        up_part = both[:, hidden_width:]
        hidden = (gate_part / (1.0 + jnp.exp(-gate_part)) * up_part).astype(bf16)
        tail = pieces[:, pair, :, pl.ds(width, wide - width)].reshape(count, wide - width)
        lane = lax.broadcasted_iota(jnp.int32, (count, wide - width), 1)
        weight = jnp.sum(jnp.where(lane == mine, tail.astype(f32), 0.0), axis=1, keepdims=True)
        tile = math.gcd(width, 1024)
        for start in range(0, width, tile):
            outputs = jnp.dot(
                hidden, down[:, pl.ds(start, tile)], preferred_element_type=f32
            ).astype(bf16)
            partial[:, :, pair, :, pl.ds(start, tile)] = (
                (outputs.astype(f32) * weight).astype(bf16).reshape(2, 2, 2, capacity, tile)
            )
        core_copy(chunk).start()

    def stage_core_sum(chunk):
        core_copy(chunk).wait_recv()
        pair = pair_of(chunk)
        to_chip[pair] = (
            partial[1 - side, core, pair].astype(f32) + from_core[1 - side, pair].astype(f32)
        ).astype(bf16)

    def return_copy(peer):
        return remote(
            final.at[peer], returned.at[me], ret_send.at[peer], ret_recv.at[me], peer, mine
        )

    def return_arrival(peer):
        return remote(
            final.at[peer], returned.at[peer], ret_send.at[peer], ret_recv.at[peer], peer, mine
        )

    def stage_final(step):
        chip_copy(step).wait_recv()
        source = flipped(me, step)
        final[source] = (
            partial[side, core, source].astype(f32)
            + from_core[side, source].astype(f32)
            + from_chip[source].astype(f32)
        ).astype(bf16)
        if step:
            return_copy(source).start()
        else:
            returned[me] = final[me]

    result_copies = [
        pltpu.make_async_copy(attended, attended_out, output_sem.at[0]),
        pltpu.make_async_copy(expert_out, expert_result, output_sem.at[1]),
    ]

    def attend():
        wait_keys(1)
        length = n * rows
        every_key = all_keys[...].reshape(length, HEAD_WIDTH)
        every_value = all_values[...].reshape(length, HEAD_WIDTH)
        key_pos = lax.broadcasted_iota(jnp.int32, (rows, length), 1)
        query_pos = lax.broadcasted_iota(jnp.int32, (rows, length), 0) + me * rows
        allowed = key_pos <= query_pos
        for head in range(heads):
            span = pl.ds(head * HEAD_WIDTH, HEAD_WIDTH)
            scores = lax.dot_general(
                queries[:, span],
                every_key,
                (((1,), (1,)), ((), ())),
                preferred_element_type=f32,
            ) * (HEAD_WIDTH ** (-0.5))
            key_gate = jnp.concatenate(
                [all_gates[peer, head : head + 1, :] for peer in range(n)], axis=1
            )
            scores = scores + column(gates[head : head + 1, :]) - key_gate
            scores = jnp.where(allowed, scores, NEGATIVE)
            top = jnp.max(scores, axis=1, keepdims=True)
            weights = jnp.where(allowed, jnp.exp(scores - top), 0.0)
            total = jnp.sum(weights, axis=1, keepdims=True)
            mixed = jnp.dot(weights.astype(bf16), every_value, preferred_element_type=f32)
            attended[:, span] = (mixed / total).astype(bf16)
        result_copies[0].start()

    stage_arrive(0)
    start_keys(4)
    stage_arrive(1)
    stage_cross(0)
    stage_arrive(2)
    stage_arrive(3)
    stage_cross(1)
    for copy in weight_copies:
        copy.wait()
    stage_compute(0)
    stage_cross(2)
    stage_arrive(4)
    stage_cross(3)
    stage_arrive(5)
    stage_cross(4)
    stage_compute(1)
    stage_core_sum(0)
    chip_copy(0).start()
    stage_arrive(6)
    stage_cross(5)
    stage_compute(2)
    stage_core_sum(2)
    chip_copy(4).start()
    chip_copy(5).start()
    stage_arrive(7)
    stage_core_sum(1)
    chip_copy(1).start()
    stage_final(4)
    stage_final(5)
    stage_cross(6)
    stage_cross(7)
    stage_final(0)
    chip_copy(2).start()
    stage_compute(3)
    stage_core_sum(3)
    chip_copy(6).start()
    chip_copy(7).start()
    chip_copy(3).start()
    wait_keys(4)
    start_keys(2)
    stage_final(1)
    wait_keys(2)
    start_keys(1)
    stage_final(2)
    stage_final(6)
    stage_final(7)
    attend()
    stage_final(3)

    for step in range(1, n):
        return_arrival(flipped(me, step)).wait_recv()
    slot_iota = lax.broadcasted_iota(jnp.int32, (rows, slots), 1).astype(f32)
    take = (slot_iota == slot).astype(f32).astype(bf16)
    expert_out[...] = jnp.dot(
        take, returned[...].reshape(slots, width), preferred_element_type=f32
    ).astype(bf16)
    result_copies[1].start()

    for step in range(1, n):
        peer = flipped(me, step)
        dispatch(peer).wait_send()
        return_copy(peer).wait_send()
    for chunk in range(chunks):
        core_copy(chunk).wait_send()
    for step in range(n):
        for which in range(3):
            forward(step, which).wait_send()
        chip_copy(step).wait_send()
    for bit in bits:
        for others in key_flips(bit):

            @pl.when(sends_keys(bit, others))
            def _():
                for which in range(3):
                    key_send_copy(which, bit, others).wait_send()
    for copy in result_copies:
        copy.wait()


def handed_on(first, second, first_out, second_out, first_held, second_held, taken, given):
    arrays = ((first, first_held, first_out), (second, second_held, second_out))
    takes = [
        pltpu.make_async_copy(source, held, taken.at[index])
        for index, (source, held, _) in enumerate(arrays)
    ]
    gives = [
        pltpu.make_async_copy(held, target, given.at[index])
        for index, (_, held, target) in enumerate(arrays)
    ]
    for copy in takes:
        copy.start()
    for take, give in zip(takes, gives):
        take.wait()
        give.start()
    for copy in gives:
        copy.wait()


def fused(
    queries, keys, values, cum_gates, expert_in, norm_gain, route_group, route_member,
    route_weight, w_gate, w_up, w_down, capacity,
):
    n = lax.axis_size("ep")
    rows, width = expert_in.shape
    hidden_width = w_gate.shape[-1]
    wide = width + 128
    bf16 = jnp.bfloat16
    vmem = pl.BlockSpec(memory_space=pltpu.VMEM)
    anywhere = pl.BlockSpec(memory_space=pl.ANY)
    dma = pltpu.SemaphoreType.DMA
    chunks = n // 2
    block = (n, capacity, width)
    inputs = (
        queries, keys, values, cum_gates.T, expert_in, norm_gain.reshape(1, width), route_group.T,
        route_member.T, route_weight.T,
    )
    results = pl.pallas_call(
        functools.partial(fused_kernel, n, capacity),
        out_shape=(
            jax.ShapeDtypeStruct(queries.shape, bf16),
            jax.ShapeDtypeStruct(expert_in.shape, bf16),
        ),
        in_specs=[anywhere] * 12,
        out_specs=(anywhere, anywhere),
        scratch_shapes=[
            *(pltpu.VMEM(array.shape, array.dtype) for array in inputs),
            pltpu.VMEM(queries.shape, bf16),
            pltpu.VMEM(expert_in.shape, bf16),
            dma((len(inputs),)),
            dma((2,)),
            pltpu.VMEM((n, capacity, wide), bf16),
            pltpu.VMEM((GROUP, n, capacity, wide), bf16),
            pltpu.VMEM((width, 2 * hidden_width), bf16),
            pltpu.VMEM((hidden_width, width), bf16),
            pltpu.VMEM((2, 2) + block, bf16),
            pltpu.VMEM((2,) + block, bf16),
            pltpu.VMEM(block, bf16),
            pltpu.VMEM(block, bf16),
            pltpu.VMEM(block, bf16),
            pltpu.VMEM(block, bf16),
            pltpu.VMEM((n,) + keys.shape, bf16),
            pltpu.VMEM((n,) + values.shape, bf16),
            pltpu.VMEM((8, rows), jnp.float32),
            pltpu.VMEM((n, 8, rows), jnp.float32),
            dma((3,)),
            dma((n,)),
            dma((n,)),
            dma((3, n)),
            dma((3, n)),
            dma((2, n)),
            dma((2, n)),
            dma((n,)),
            dma((n,)),
            dma((3, n)),
            dma((3, n)),
        ],
        compiler_params=pltpu.CompilerParams(
            collective_id=0, has_side_effects=True, vmem_limit_bytes=62 * 1024 * 1024
        ),
        name="fused",
    )(
        *inputs, w_gate, w_up, w_down,
    )
    return pl.pallas_call(
        handed_on,
        out_shape=tuple(jax.ShapeDtypeStruct(result.shape, bf16) for result in results),
        in_specs=[anywhere, anywhere],
        out_specs=(anywhere, anywhere),
        scratch_shapes=[
            *(pltpu.VMEM(result.shape, bf16) for result in results),
            dma((2,)),
            dma((2,)),
        ],
        name="handed_on",
    )(*results)


def per_device(
    queries,
    keys,
    values,
    cum_gates,
    expert_in,
    norm_gain,
    route_group,
    route_member,
    route_weight,
    w_gate,
    w_up,
    w_down,
):
    ep_size = lax.axis_size("ep")
    count_rows = expert_in.shape[0]
    capacity = max(2, (3 * count_rows + 2 * ep_size - 1) // (2 * ep_size))
    fits = keys.shape[1] == HEAD_WIDTH and count_rows == queries.shape[0] == HEAD_WIDTH
    if lax.axis_size("tp") == GROUP and ep_size == 8 and capacity % 8 == 0 and fits:
        return fused(
            queries, keys, values, cum_gates, expert_in, norm_gain, route_group, route_member,
            route_weight, w_gate, w_up, w_down, capacity,
        )
    attended = attention_half(queries, keys, values, cum_gates)
    expert_out = expert_half(
        expert_in, norm_gain, route_group, route_member, route_weight, w_gate, w_up, w_down
    )
    return (attended, expert_out)


def solution(mesh):
    return jax.shard_map(
        per_device,
        mesh=mesh,
        in_specs=(
            P("ep", "tp"),
            P("ep", "tp"),
            P("ep", "tp"),
            P("ep", "tp"),
            P(("ep", "tp"), None),
            P(),
            P(("ep", "tp"), None),
            P(("ep", "tp"), None),
            P(("ep", "tp"), None),
            P(("ep", "tp"), None, None),
            P(("ep", "tp"), None, None),
            P(("ep", "tp"), None, None),
        ),
        out_specs=(P("ep", "tp"), P(("ep", "tp"), None)),
        check_vma=False,
    )
```

profile of v0, /device:TPU:0, one launch (start us, length us, event | category | flops | bytes accessed | tf_op | source)
XLA Modules:
  0.0 98.1 jit_solution(8907465055933108958)
XLA Ops:
  0.6 95.2 %fused.1 = (bf16[128,512]{1,0:T(8,128)(2,1)}, bf16[128,4096]{1,0:T(8,128)(2,1)}) custom-call(bf16[128,512]{1,0:T(8,128)(2,1)} %queries_in.1, bf16[128,128]{1,0:T(8,128)(2,1)} %keys_in.1, bf16[128,128]{1,0:T(8,128)(2,1)} %values_in.1, f32[4,128]{1,0:T(4,128)} %bitcast.6, bf16[128,4096]{1,0:T(8,128)(2,1)} %expert_rows.1, f32[1,4096]{1,0:T(1,128)} %bitcast.5, ...), custom_call_target="tpu_custom_call" | custom-call | tf_op jit(solution)/shard_map/fused/pallas_call | solution.py:707
  95.8 2.3 %handed_on.1 = (bf16[128,512]{1,0:T(8,128)(2,1)}, bf16[128,4096]{1,0:T(8,128)(2,1)}) custom-call(bf16[128,512]{1,0:T(8,128)(2,1)} %get-tuple-element.4.first, bf16[128,4096]{1,0:T(8,128)(2,1)} %get-tuple-element.5.second), custom_call_target="tpu_custom_call" | custom-call | tf_op jit(solution)/shard_map/handed_on/pallas_call | solution.py:754
where the time goes:
time: 98.3 us; the launch traced here: 98.1 us
  Pallas kernels  97.5 us (99%)
    pallas_call x1, Pallas kernels, fused(): pl.pallas_call(functools.partial(fused_kernel, n, capacity), out_shape=(j...  95.2 us
    pallas_call x1, Pallas kernels, fused(): pl.pallas_call(handed_on, out_shape=tuple((jax.ShapeDtypeStruct(result.sh...  2.31 us

commit v1 on v0

--- a/solution.py
+++ b/solution.py
@@ -1,4 +1,5 @@
 import functools
+import itertools
 import math
 
 import jax
@@ -11,6 +12,153 @@
 HEAD_WIDTH = 128
 GROUP = 4
 TOP = 2
+
+
+OUTER, INNER, BOTH = range(3)
+ARRIVE, CROSS, COMPUTE, CORE_SUM, CHIP, FINAL, KEYS, WEIGHTS = range(8)
+HALVES = 2
+CHUNKS = ((4, 5), (6, 7), (2, 3), (0, 1))
+DISPATCH = ((6, 4, 5, 2, 1, 7, 3), (6, 4, 5, 2, 1, 7, 3))
+PLAN = (
+    (BOTH, ARRIVE, 0, 1),
+    (BOTH, ARRIVE, 0, 0),
+    (BOTH, ARRIVE, 1, 0),
+    (BOTH, ARRIVE, 1, 1),
+    (OUTER, ARRIVE, 6, 1),
+    (OUTER, ARRIVE, 2, 1),
+    (INNER, ARRIVE, 4, 0),
+    (INNER, ARRIVE, 4, 1),
+    (INNER, ARRIVE, 5, 0),
+    (INNER, ARRIVE, 5, 1),
+    (INNER, CROSS, 4, 1),
+    (BOTH, CROSS, 0, 1),
+    (OUTER, CROSS, 1, 0),
+    (INNER, ARRIVE, 2, 0),
+    (INNER, CROSS, 4, 0),
+    (INNER, CROSS, 0, 0),
+    (INNER, CROSS, 5, 1),
+    (INNER, CROSS, 5, 0),
+    (BOTH, ARRIVE, 6, 0),
+    (INNER, ARRIVE, 2, 1),
+    (INNER, ARRIVE, 6, 1),
+    (INNER, WEIGHTS, 0, 0),
+    (INNER, COMPUTE, 0, 0),
+    (INNER, CROSS, 1, 1),
+    (INNER, CORE_SUM, 0, 0),
+    (INNER, CROSS, 2, 0),
+    (INNER, CROSS, 2, 1),
+    (INNER, CHIP, 4, 0),
+    (BOTH, ARRIVE, 3, 0),
+    (INNER, CROSS, 1, 0),
+    (BOTH, ARRIVE, 3, 1),
+    (OUTER, CROSS, 0, 0),
+    (OUTER, CROSS, 2, 1),
+    (OUTER, CROSS, 6, 1),
+    (OUTER, ARRIVE, 2, 0),
+    (OUTER, CROSS, 1, 1),
+    (BOTH, CROSS, 6, 0),
+    (OUTER, WEIGHTS, 0, 0),
+    (INNER, CORE_SUM, 0, 1),
+    (INNER, FINAL, 4, 0),
+    (INNER, CROSS, 6, 1),
+    (INNER, CHIP, 5, 1),
+    (INNER, CHIP, 4, 1),
+    (BOTH, COMPUTE, 3, 0),
+    (OUTER, ARRIVE, 7, 0),
+    (OUTER, CROSS, 3, 1),
+    (BOTH, ARRIVE, 7, 1),
+    (OUTER, ARRIVE, 4, 0),
+    (OUTER, CROSS, 7, 0),
+    (OUTER, ARRIVE, 4, 1),
+    (OUTER, CROSS, 7, 1),
+    (INNER, FINAL, 5, 1),
+    (INNER, CHIP, 5, 0),
+    (INNER, CROSS, 3, 0),
+    (INNER, CROSS, 3, 1),
+    (INNER, ARRIVE, 7, 0),
+    (INNER, CORE_SUM, 3, 1),
+    (INNER, COMPUTE, 2, 0),
+    (BOTH, CORE_SUM, 3, 0),
+    (OUTER, CROSS, 3, 0),
+    (OUTER, ARRIVE, 5, 0),
+    (INNER, CORE_SUM, 2, 1),
+    (INNER, CROSS, 7, 1),
+    (INNER, FINAL, 4, 1),
+    (INNER, CHIP, 1, 1),
+    (INNER, CHIP, 1, 0),
+    (INNER, CROSS, 7, 0),
+    (INNER, CORE_SUM, 2, 0),
+    (INNER, CHIP, 3, 1),
+    (INNER, KEYS, 4, 0),
+    (BOTH, COMPUTE, 1, 0),
+    (OUTER, ARRIVE, 5, 1),
+    (OUTER, CROSS, 2, 0),
+    (OUTER, CORE_SUM, 1, 1),
+    (BOTH, CORE_SUM, 1, 0),
+    (OUTER, CHIP, 6, 0),
+    (OUTER, CHIP, 7, 1),
+    (OUTER, COMPUTE, 2, 0),
+    (OUTER, CORE_SUM, 2, 0),
+    (OUTER, CROSS, 5, 1),
+    (OUTER, CROSS, 4, 1),
+    (OUTER, CROSS, 5, 0),
+    (OUTER, CHIP, 6, 1),
+    (OUTER, CHIP, 7, 0),
+    (OUTER, CROSS, 4, 0),
+    (OUTER, FINAL, 6, 0),
+    (OUTER, COMPUTE, 0, 0),
+    (OUTER, CORE_SUM, 2, 1),
+    (OUTER, CORE_SUM, 0, 1),
+    (OUTER, CHIP, 5, 1),
+    (OUTER, CORE_SUM, 0, 0),
+    (OUTER, FINAL, 6, 1),
+    (OUTER, CHIP, 5, 0),
+    (OUTER, CHIP, 4, 1),
+    (OUTER, FINAL, 7, 1),
+    (OUTER, CHIP, 3, 1),
+    (OUTER, CHIP, 4, 0),
+    (OUTER, CHIP, 1, 0),
+    (OUTER, CORE_SUM, 3, 1),
+    (OUTER, KEYS, 4, 0),
+    (OUTER, FINAL, 7, 0),
+    (OUTER, FINAL, 5, 1),
+    (INNER, FINAL, 1, 1),
+    (INNER, CHIP, 3, 0),
+    (BOTH, FINAL, 5, 0),
+    (OUTER, FINAL, 4, 1),
+    (OUTER, CHIP, 2, 0),
+    (OUTER, CHIP, 2, 1),
+    (BOTH, FINAL, 3, 1),
+    (OUTER, FINAL, 4, 0),
+    (OUTER, CHIP, 1, 1),
+    (INNER, CHIP, 2, 0),
+    (INNER, CORE_SUM, 1, 1),
+    (INNER, CHIP, 2, 1),
+    (INNER, CHIP, 7, 0),
+    (INNER, CHIP, 7, 1),
+    (INNER, FINAL, 3, 0),
+    (INNER, CHIP, 6, 1),
+    (INNER, CHIP, 6, 0),
+    (INNER, CHIP, 0, 0),
+    (BOTH, KEYS, 2, 0),
+    (INNER, FINAL, 7, 0),
+    (INNER, FINAL, 7, 1),
+    (INNER, FINAL, 6, 1),
+    (INNER, FINAL, 2, 0),
+    (BOTH, FINAL, 1, 0),
+    (OUTER, CHIP, 3, 0),
+    (OUTER, CHIP, 0, 1),
+    (INNER, FINAL, 6, 0),
+    (BOTH, FINAL, 2, 1),
+    (OUTER, CHIP, 0, 0),
+    (OUTER, FINAL, 2, 0),
+    (OUTER, FINAL, 3, 0),
+    (OUTER, FINAL, 1, 1),
+    (OUTER, FINAL, 0, 1),
+    (INNER, CHIP, 0, 1),
+    (BOTH, FINAL, 0, 0),
+    (INNER, FINAL, 0, 1),
+)
 
 
 NEGATIVE = -1e30
@@ -249,8 +397,10 @@
     disp_recv,
     fwd_send,
     fwd_recv,
-    part_send,
-    part_recv,
+    core_send,
+    core_recv,
+    chip_send,
+    chip_recv,
     ret_send,
     ret_recv,
     key_send,
@@ -260,7 +410,6 @@
     rows, width = expert_in.shape
     hidden_width = down.shape[0]
     wide = pieces.shape[-1]
-    chunks = n // 2
     me = lax.axis_index("ep")
     mine = lax.axis_index("tp")
     core = mine % 2
@@ -389,18 +538,45 @@
 
     pl.semaphore_wait(barrier, n + 1)
 
-    def dispatch(peer):
+    half = width // HALVES
+    inner = ((me // 2 + 1) // 2) % 2
+
+    def columns(part):
+        return pl.ds(part * half, half + (wide - width if part == HALVES - 1 else 0))
+
+    def narrow(part):
+        return pl.ds(part * half, half)
+
+    def dispatch(peer, part):
         return remote(
-            send.at[peer], pieces.at[mine, me], disp_send.at[peer], disp_recv.at[me], peer, mine
-        )
-
-    def arrival(peer):
+            send.at[peer, :, columns(part)],
+            pieces.at[mine, me, :, columns(part)],
+            disp_send.at[peer, part],
+            disp_recv.at[me, part],
+            peer,
+            mine,
+        )
+
+    def arrival(peer, part):
         return remote(
-            send.at[peer], pieces.at[mine, peer], disp_send.at[peer], disp_recv.at[peer], peer, mine
-        )
-
-    for step in range(1, n):
-        dispatch(flipped(me, step)).start()
+            send.at[peer, :, columns(part)],
+            pieces.at[mine, peer, :, columns(part)],
+            disp_send.at[peer, part],
+            disp_recv.at[peer, part],
+            peer,
+            mine,
+        )
+
+    def send_rows(order):
+        for step in order:
+            for part in range(HALVES):
+                dispatch(flipped(me, step), part).start()
+
+    if DISPATCH[0] == DISPATCH[1]:
+        send_rows(DISPATCH[0])
+    else:
+        for kind in range(2):
+            pl.when(inner == kind)(functools.partial(send_rows, DISPATCH[kind]))
     pieces[mine, me] = send[me]
 
     shared = (all_keys, all_values, all_gates)
@@ -452,61 +628,75 @@
                     key_send_copy(which, bit, others).start()
 
     def pair_of(chunk):
-        return pl.ds(flipped(me // 2, chunk) * 2, 2)
-
-    def forward(step, which):
-        part = pieces.at[across if which == 2 else mine, flipped(me, step)]
+        steps = CHUNKS[chunk]
+        if len(steps) == 1:
+            return pl.ds(flipped(me, steps[0]), 1)
+        return pl.ds(flipped(me // 2, steps[0] // 2) * 2, 2)
+
+    def forward(step, which, part):
+        block = pieces.at[across if which == 2 else mine, flipped(me, step), :, columns(part)]
         return remote(
-            part,
-            part,
-            fwd_send.at[which, step],
-            fwd_recv.at[which, step],
+            block,
+            block,
+            fwd_send.at[which, step, part],
+            fwd_recv.at[which, step, part],
             me,
             across if which == 1 else twin,
         )
 
-    def forwarded(step, which):
-        part = pieces.at[(twin, across, diagonal)[which], flipped(me, step)]
-        return remote(part, part, fwd_send.at[which, step], fwd_recv.at[which, step], me, twin)
-
-    def stage_arrive(step):
+    def forwarded(step, which, part):
+        block = pieces.at[
+            (twin, across, diagonal)[which], flipped(me, step), :, columns(part)
+        ]
+        return remote(
+            block,
+            block,
+            fwd_send.at[which, step, part],
+            fwd_recv.at[which, step, part],
+            me,
+            twin,
+        )
+
+    def stage_arrive(step, part):
         if step:
-            arrival(flipped(me, step)).wait_recv()
-        forward(step, 1).start()
-        forward(step, 0).start()
-
-    def stage_cross(step):
-        forwarded(step, 1).wait_recv()
-        forward(step, 2).start()
-
-    def core_copy(chunk):
+            arrival(flipped(me, step), part).wait_recv()
+        forward(step, 1, part).start()
+        forward(step, 0, part).start()
+
+    def stage_cross(step, part):
+        forwarded(step, 1, part).wait_recv()
+        forward(step, 2, part).start()
+
+    def core_copy(chunk, part):
         pair = pair_of(chunk)
         return remote(
-            partial.at[:, 1 - core, pair],
-            from_core.at[:, pair],
-            part_send.at[0, chunk],
-            part_recv.at[0, chunk],
+            partial.at[:, 1 - core, pair, :, narrow(part)],
+            from_core.at[:, pair, :, narrow(part)],
+            core_send.at[chunk, part],
+            core_recv.at[chunk, part],
             me,
             twin,
         )
 
-    def chip_copy(step):
+    def chip_copy(step, part):
         source = flipped(me, step)
         return remote(
-            to_chip.at[source],
-            from_chip.at[source],
-            part_send.at[1, step],
-            part_recv.at[1, step],
+            to_chip.at[source, :, narrow(part)],
+            from_chip.at[source, :, narrow(part)],
+            chip_send.at[step, part],
+            chip_recv.at[step, part],
             me,
             across,
         )
 
-    def stage_compute(chunk):
-        for step in (chunk * 2, chunk * 2 + 1):
-            forwarded(step, 0).wait_recv()
-            forwarded(step, 2).wait_recv()
+    def stage_compute(chunk, _):
+        for step in CHUNKS[chunk]:
+            for part in range(HALVES):
+                forwarded(step, 0, part).wait_recv()
+                forwarded(step, 2, part).wait_recv()
         pair = pair_of(chunk)
-        count = 4 * 2 * capacity
+        blocks = len(CHUNKS[chunk])
+        count = GROUP * blocks * capacity
         held = pieces[:, pair, :, pl.ds(0, width)].reshape(count, width)
         both = jnp.dot(held, gate_up[...], preferred_element_type=f32)
         gate_part = both[:, :hidden_width]
@@ -515,45 +705,65 @@
         tail = pieces[:, pair, :, pl.ds(width, wide - width)].reshape(count, wide - width)
         lane = lax.broadcasted_iota(jnp.int32, (count, wide - width), 1)
         weight = jnp.sum(jnp.where(lane == mine, tail.astype(f32), 0.0), axis=1, keepdims=True)
-        tile = math.gcd(width, 1024)
-        for start in range(0, width, tile):
-            outputs = jnp.dot(
-                hidden, down[:, pl.ds(start, tile)], preferred_element_type=f32
-            ).astype(bf16)
-            partial[:, :, pair, :, pl.ds(start, tile)] = (
-                (outputs.astype(f32) * weight).astype(bf16).reshape(2, 2, 2, capacity, tile)
-            )
-        core_copy(chunk).start()
-
-    def stage_core_sum(chunk):
-        core_copy(chunk).wait_recv()
+        tile = math.gcd(half, 1024)
+        for part in range(HALVES):
+            for start in range(part * half, (part + 1) * half, tile):
+                outputs = jnp.dot(
+                    hidden, down[:, pl.ds(start, tile)], preferred_element_type=f32
+                ).astype(bf16)
+                partial[:, :, pair, :, pl.ds(start, tile)] = (
+                    (outputs.astype(f32) * weight)
+                    .astype(bf16)
+                    .reshape(2, 2, blocks, capacity, tile)
+                )
+            core_copy(chunk, part).start()
+
+    def stage_core_sum(chunk, part):
+        core_copy(chunk, part).wait_recv()
         pair = pair_of(chunk)
-        to_chip[pair] = (
-            partial[1 - side, core, pair].astype(f32) + from_core[1 - side, pair].astype(f32)
+        span = narrow(part)
+        to_chip[pair, :, span] = (
+            partial[1 - side, core, pair, :, span].astype(f32)
+            + from_core[1 - side, pair, :, span].astype(f32)
         ).astype(bf16)
 
-    def return_copy(peer):
+    def stage_chip(step, part):
+        chip_copy(step, part).start()
+
+    def return_copy(peer, part):
         return remote(
-            final.at[peer], returned.at[me], ret_send.at[peer], ret_recv.at[me], peer, mine
-        )
-
-    def return_arrival(peer):
+            final.at[peer, :, narrow(part)],
+            returned.at[me, :, narrow(part)],
+            ret_send.at[peer, part],
+            ret_recv.at[me, part],
+            peer,
+            mine,
+        )
+
+    def return_arrival(peer, part):
         return remote(
-            final.at[peer], returned.at[peer], ret_send.at[peer], ret_recv.at[peer], peer, mine
-        )
-
-    def stage_final(step):
-        chip_copy(step).wait_recv()
+            final.at[peer, :, narrow(part)],
+            returned.at[peer, :, narrow(part)],
+            ret_send.at[peer, part],
+            ret_recv.at[peer, part],
+            peer,
+            mine,
+        )
+
+    def stage_final(step, part):
+        chip_copy(step, part).wait_recv()
         source = flipped(me, step)
-        final[source] = (
-            partial[side, core, source].astype(f32)
-            + from_core[side, source].astype(f32)
-            + from_chip[source].astype(f32)
+        span = narrow(part)
+        total = (
+            partial[side, core, source, :, span].astype(f32)
+            + from_core[side, source, :, span].astype(f32)
+            + from_chip[source, :, span].astype(f32)
         ).astype(bf16)
         if step:
-            return_copy(source).start()
+            final[source, :, span] = total
+            return_copy(source, part).start()
         else:
-            returned[me] = final[me]
+            returned[me, :, span] = total
 
     result_copies = [
         pltpu.make_async_copy(attended, attended_out, output_sem.at[0]),
@@ -588,57 +798,34 @@
             attended[:, span] = (mixed / total).astype(bf16)
         result_copies[0].start()
 
-    stage_arrive(0)
+    def keys_on(bit, _):
+        wait_keys(bit)
+        start_keys(bit // 2)
+
+    def weights_in(*_):
+        for copy in weight_copies:
+            copy.wait()
+
+    stages = (
+        stage_arrive, stage_cross, stage_compute, stage_core_sum, stage_chip, stage_final,
+        keys_on, weights_in,
+    )
+
+    def run(actions):
+        for _, kind, number, part in actions:
+            stages[kind](number, part)
+
     start_keys(4)
-    stage_arrive(1)
-    stage_cross(0)
-    stage_arrive(2)
-    stage_arrive(3)
-    stage_cross(1)
-    for copy in weight_copies:
-        copy.wait()
-    stage_compute(0)
-    stage_cross(2)
-    stage_arrive(4)
-    stage_cross(3)
-    stage_arrive(5)
-    stage_cross(4)
-    stage_compute(1)
-    stage_core_sum(0)
-    chip_copy(0).start()
-    stage_arrive(6)
-    stage_cross(5)
-    stage_compute(2)
-    stage_core_sum(2)
-    chip_copy(4).start()
-    chip_copy(5).start()
-    stage_arrive(7)
-    stage_core_sum(1)
-    chip_copy(1).start()
-    stage_final(4)
-    stage_final(5)
-    stage_cross(6)
-    stage_cross(7)
-    stage_final(0)
-    chip_copy(2).start()
-    stage_compute(3)
-    stage_core_sum(3)
-    chip_copy(6).start()
-    chip_copy(7).start()
-    chip_copy(3).start()
-    wait_keys(4)
-    start_keys(2)
-    stage_final(1)
-    wait_keys(2)
-    start_keys(1)
-    stage_final(2)
-    stage_final(6)
-    stage_final(7)
+    for who, actions in itertools.groupby(PLAN, lambda action: action[0]):
+        if who == BOTH:
+            run(actions)
+        else:
+            pl.when(inner == who)(functools.partial(run, tuple(actions)))
     attend()
-    stage_final(3)
 
     for step in range(1, n):
-        return_arrival(flipped(me, step)).wait_recv()
+        for part in range(HALVES):
+            return_arrival(flipped(me, step), part).wait_recv()
     slot_iota = lax.broadcasted_iota(jnp.int32, (rows, slots), 1).astype(f32)
     take = (slot_iota == slot).astype(f32).astype(bf16)
     expert_out[...] = jnp.dot(
@@ -648,14 +835,16 @@
 
     for step in range(1, n):
         peer = flipped(me, step)
-        dispatch(peer).wait_send()
-        return_copy(peer).wait_send()
-    for chunk in range(chunks):
-        core_copy(chunk).wait_send()
-    for step in range(n):
-        for which in range(3):
-            forward(step, which).wait_send()
-        chip_copy(step).wait_send()
+        for part in range(HALVES):
+            dispatch(peer, part).wait_send()
+            return_copy(peer, part).wait_send()
+    for part in range(HALVES):
+        for chunk in range(len(CHUNKS)):
+            core_copy(chunk, part).wait_send()
+        for step in range(n):
+            for which in range(3):
+                forward(step, which, part).wait_send()
+            chip_copy(step, part).wait_send()
     for bit in bits:
         for others in key_flips(bit):
 
@@ -698,7 +887,6 @@
     vmem = pl.BlockSpec(memory_space=pltpu.VMEM)
     anywhere = pl.BlockSpec(memory_space=pl.ANY)
     dma = pltpu.SemaphoreType.DMA
-    chunks = n // 2
     block = (n, capacity, width)
     inputs = (
         queries, keys, values, cum_gates.T, expert_in, norm_gain.reshape(1, width), route_group.T,
@@ -733,14 +921,16 @@
             pltpu.VMEM((8, rows), jnp.float32),
             pltpu.VMEM((n, 8, rows), jnp.float32),
             dma((3,)),
-            dma((n,)),
-            dma((n,)),
-            dma((3, n)),
-            dma((3, n)),
-            dma((2, n)),
-            dma((2, n)),
-            dma((n,)),
-            dma((n,)),
+            dma((n, HALVES)),
+            dma((n, HALVES)),
+            dma((3, n, HALVES)),
+            dma((3, n, HALVES)),
+            dma((len(CHUNKS), HALVES)),
+            dma((len(CHUNKS), HALVES)),
+            dma((n, HALVES)),
+            dma((n, HALVES)),
+            dma((n, HALVES)),
+            dma((n, HALVES)),
             dma((3, n)),
             dma((3, n)),
         ],

time: 98.3 us -> 89.3 us (0.908)
  Pallas kernels: 97.5 us -> 88.3 us
    pallas_call x1, Pallas kernels: 95.2 us -> 86 us  [fused(): pl.pallas_call(functools.partial(fused_kernel, n, capacity), out_shape=(j...]
where the time goes in v1:
time: 89.3 us; the launch traced here: 89.1 us
  Pallas kernels  88.3 us (99%)
    pallas_call x1, Pallas kernels, fused(): pl.pallas_call(functools.partial(fused_kernel, n, capacity), out_shape=(j...  86 us
    pallas_call x1, Pallas kernels, fused(): pl.pallas_call(handed_on, out_shape=tuple((jax.ShapeDtypeStruct(result.sh...  2.31 us

profile of v1, /device:TPU:0, one launch (start us, length us, event | category | flops | bytes accessed | tf_op | source)
XLA Modules:
  0.0 89.1 jit_solution(4772153009881501777)
XLA Ops:
  0.6 86.0 %fused.1 = (bf16[128,512]{1,0:T(8,128)(2,1)}, bf16[128,4096]{1,0:T(8,128)(2,1)}) custom-call(bf16[128,512]{1,0:T(8,128)(2,1)} %queries_in.1, bf16[128,128]{1,0:T(8,128)(2,1)} %keys_in.1, bf16[128,128]{1,0:T(8,128)(2,1)} %values_in.1, f32[4,128]{1,0:T(4,128)} %bitcast.6, bf16[128,4096]{1,0:T(8,128)(2,1)} %expert_rows.1, f32[1,4096]{1,0:T(1,128)} %bitcast.5, ...), custom_call_target="tpu_custom_call" | custom-call | tf_op jit(solution)/shard_map/fused/pallas_call | solution.py:895
  86.7 2.3 %handed_on.1 = (bf16[128,512]{1,0:T(8,128)(2,1)}, bf16[128,4096]{1,0:T(8,128)(2,1)}) custom-call(bf16[128,512]{1,0:T(8,128)(2,1)} %get-tuple-element.4.first, bf16[128,4096]{1,0:T(8,128)(2,1)} %get-tuple-element.5.second), custom_call_target="tpu_custom_call" | custom-call | tf_op jit(solution)/shard_map/handed_on/pallas_call | solution.py:944

commit v2 on v1

--- a/solution.py
+++ b/solution.py
@@ -15,7 +15,7 @@
 
 
 OUTER, INNER, BOTH = range(3)
-ARRIVE, CROSS, COMPUTE, CORE_SUM, CHIP, FINAL, KEYS, WEIGHTS = range(8)
+ARRIVE, CROSS, COMPUTE, CORE_SUM, CHIP, FINAL, KEYS, WEIGHTS, ATTEND, DRAIN = range(10)
 HALVES = 2
 CHUNKS = ((4, 5), (6, 7), (2, 3), (0, 1))
 DISPATCH = ((6, 4, 5, 2, 1, 7, 3), (6, 4, 5, 2, 1, 7, 3))
@@ -81,6 +81,7 @@
     (BOTH, CORE_SUM, 3, 0),
     (OUTER, CROSS, 3, 0),
     (OUTER, ARRIVE, 5, 0),
+    (INNER, KEYS, 4, 0),
     (INNER, CORE_SUM, 2, 1),
     (INNER, CROSS, 7, 1),
     (INNER, FINAL, 4, 1),
@@ -89,7 +90,6 @@
     (INNER, CROSS, 7, 0),
     (INNER, CORE_SUM, 2, 0),
     (INNER, CHIP, 3, 1),
-    (INNER, KEYS, 4, 0),
     (BOTH, COMPUTE, 1, 0),
     (OUTER, ARRIVE, 5, 1),
     (OUTER, CROSS, 2, 0),
@@ -107,6 +107,7 @@
     (OUTER, CROSS, 4, 0),
     (OUTER, FINAL, 6, 0),
     (OUTER, COMPUTE, 0, 0),
+    (OUTER, KEYS, 4, 0),
     (OUTER, CORE_SUM, 2, 1),
     (OUTER, CORE_SUM, 0, 1),
     (OUTER, CHIP, 5, 1),
@@ -119,7 +120,6 @@
     (OUTER, CHIP, 4, 0),
     (OUTER, CHIP, 1, 0),
     (OUTER, CORE_SUM, 3, 1),
-    (OUTER, KEYS, 4, 0),
     (OUTER, FINAL, 7, 0),
     (OUTER, FINAL, 5, 1),
     (INNER, FINAL, 1, 1),
@@ -128,6 +128,7 @@
     (OUTER, FINAL, 4, 1),
     (OUTER, CHIP, 2, 0),
     (OUTER, CHIP, 2, 1),
+    (OUTER, KEYS, 2, 0),
     (BOTH, FINAL, 3, 1),
     (OUTER, FINAL, 4, 0),
     (OUTER, CHIP, 1, 1),
@@ -140,7 +141,7 @@
     (INNER, CHIP, 6, 1),
     (INNER, CHIP, 6, 0),
     (INNER, CHIP, 0, 0),
-    (BOTH, KEYS, 2, 0),
+    (INNER, KEYS, 2, 0),
     (INNER, FINAL, 7, 0),
     (INNER, FINAL, 7, 1),
     (INNER, FINAL, 6, 1),
@@ -148,14 +149,17 @@
     (BOTH, FINAL, 1, 0),
     (OUTER, CHIP, 3, 0),
     (OUTER, CHIP, 0, 1),
+    (INNER, ATTEND, 0, 0),
     (INNER, FINAL, 6, 0),
     (BOTH, FINAL, 2, 1),
     (OUTER, CHIP, 0, 0),
     (OUTER, FINAL, 2, 0),
+    (OUTER, ATTEND, 0, 0),
     (OUTER, FINAL, 3, 0),
     (OUTER, FINAL, 1, 1),
+    (INNER, CHIP, 0, 1),
+    (BOTH, DRAIN, 0, 0),
     (OUTER, FINAL, 0, 1),
-    (INNER, CHIP, 0, 1),
     (BOTH, FINAL, 0, 0),
     (INNER, FINAL, 0, 1),
 )
@@ -348,6 +352,29 @@
     return result
 
 
+def column_of(rows):
+    row_i = lax.broadcasted_iota(jnp.int32, (rows, rows), 0)
+    same = row_i == lax.broadcasted_iota(jnp.int32, (rows, rows), 1)
+
+    def column(row):
+        return jnp.sum(jnp.where(same, row.astype(jnp.float32), 0.0), axis=1, keepdims=True)
+
+    return column
+
+
+def slots_of(route_group, capacity):
+    f32, bf16 = jnp.float32, jnp.bfloat16
+    rows = route_group.shape[1]
+    lanes = lax.broadcasted_iota(jnp.int32, (rows, 128), 1)
+    row_i = lax.broadcasted_iota(jnp.int32, (rows, rows), 0)
+    earlier = (lax.broadcasted_iota(jnp.int32, (rows, rows), 1) < row_i).astype(bf16)
+    group = column_of(rows)(route_group[...])
+    match = (group == lanes.astype(f32)).astype(f32)
+    ranks = jnp.dot(earlier, match.astype(bf16), preferred_element_type=f32)
+    rank_within = jnp.sum(ranks * match, axis=1, keepdims=True)
+    return group * float(capacity) + rank_within
+
+
 def fused_kernel(
     n,
     capacity,
@@ -364,7 +391,7 @@
     w_up,
     w_down,
     attended_out,
-    expert_result,
+    returned_out,
     queries,
     keys,
     values,
@@ -375,7 +402,6 @@
     route_member,
     route_weight,
     attended,
-    expert_out,
     input_sem,
     output_sem,
     send,
@@ -387,7 +413,6 @@
     to_chip,
     from_chip,
     final,
-    returned,
     all_keys,
     all_values,
     own_gates,
@@ -397,6 +422,7 @@
     disp_recv,
     fwd_send,
     fwd_recv,
+    both_recv,
     core_send,
     core_recv,
     chip_send,
@@ -473,25 +499,15 @@
             device_id_type=pl.DeviceIdType.MESH,
         )
 
-    for copy in weight_copies:
-        copy.start()
-    for copy in input_copies[:3]:
+    for copy in input_copies[:5]:
         copy.wait()
 
     lanes = lax.broadcasted_iota(jnp.int32, (rows, 128), 1)
-    row_i = lax.broadcasted_iota(jnp.int32, (rows, rows), 0)
-    col_i = lax.broadcasted_iota(jnp.int32, (rows, rows), 1)
-    earlier = (col_i < row_i).astype(bf16)
-    same = row_i == col_i
-
-    def column(row):
-        return jnp.sum(jnp.where(same, row.astype(f32), 0.0), axis=1, keepdims=True)
-
-    group = column(route_group[...])
-    match = (group == lanes.astype(f32)).astype(f32)
-    ranks = jnp.dot(earlier, match.astype(bf16), preferred_element_type=f32)
-    rank_within = jnp.sum(ranks * match, axis=1, keepdims=True)
-    slot = group * float(capacity) + rank_within
+    column = column_of(rows)
+    slot = slots_of(route_group, capacity)
+    same = lax.broadcasted_iota(jnp.int32, (rows, rows), 0) == lax.broadcasted_iota(
+        jnp.int32, (rows, rows), 1
+    )
     slot_row = jnp.sum(jnp.where(same, slot, 0.0), axis=0, keepdims=True)
     slots = n * capacity
     place = (
@@ -504,8 +520,6 @@
             column(route_weight[rank_index : rank_index + 1, :]),
             0.0,
         )
-    for copy in input_copies[3:5]:
-        copy.wait()
     floats = expert_in[...].astype(f32)
     scale = lax.rsqrt(jnp.mean(floats * floats, axis=-1, keepdims=True) + EPSILON)
     normed = (floats * scale * gain[...]).astype(bf16)
@@ -519,6 +533,50 @@
         .astype(bf16)
         .reshape(n, capacity, wide - width)
     )
+    pl.semaphore_wait(barrier, n + 1)
+
+    half = width // HALVES
+    inner = ((me // 2 + 1) // 2) % 2
+
+    def columns(part):
+        return pl.ds(part * half, half + (wide - width if part == HALVES - 1 else 0))
+
+    def narrow(part):
+        return pl.ds(part * half, half)
+
+    def dispatch(peer, part):
+        return remote(
+            send.at[peer, :, columns(part)],
+            pieces.at[mine, me, :, columns(part)],
+            disp_send.at[0],
+            disp_recv.at[me, part],
+            peer,
+            mine,
+        )
+
+    def arrival(peer, part):
+        return remote(
+            send.at[peer, :, columns(part)],
+            pieces.at[mine, peer, :, columns(part)],
+            disp_send.at[0],
+            disp_recv.at[peer, part],
+            peer,
+            mine,
+        )
+
+    def send_rows(order):
+        for step in order:
+            for part in range(HALVES):
+                dispatch(flipped(me, step), part).start()
+
+    if DISPATCH[0] == DISPATCH[1]:
+        send_rows(DISPATCH[0])
+    else:
+        for kind in range(2):
+            pl.when(inner == kind)(functools.partial(send_rows, DISPATCH[kind]))
+    for copy in weight_copies:
+        copy.start()
+    pieces[mine, me] = send[me]
     for copy in input_copies[5:]:
         copy.wait()
     heads = gates.shape[0]
@@ -536,48 +594,6 @@
     all_keys[me] = keys[...]
     all_values[me] = values[...]
 
-    pl.semaphore_wait(barrier, n + 1)
-
-    half = width // HALVES
-    inner = ((me // 2 + 1) // 2) % 2
-
-    def columns(part):
-        return pl.ds(part * half, half + (wide - width if part == HALVES - 1 else 0))
-
-    def narrow(part):
-        return pl.ds(part * half, half)
-
-    def dispatch(peer, part):
-        return remote(
-            send.at[peer, :, columns(part)],
-            pieces.at[mine, me, :, columns(part)],
-            disp_send.at[peer, part],
-            disp_recv.at[me, part],
-            peer,
-            mine,
-        )
-
-    def arrival(peer, part):
-        return remote(
-            send.at[peer, :, columns(part)],
-            pieces.at[mine, peer, :, columns(part)],
-            disp_send.at[peer, part],
-            disp_recv.at[peer, part],
-            peer,
-            mine,
-        )
-
-    def send_rows(order):
-        for step in order:
-            for part in range(HALVES):
-                dispatch(flipped(me, step), part).start()
-
-    if DISPATCH[0] == DISPATCH[1]:
-        send_rows(DISPATCH[0])
-    else:
-        for kind in range(2):
-            pl.when(inner == kind)(functools.partial(send_rows, DISPATCH[kind]))
-    pieces[mine, me] = send[me]
 
     shared = (all_keys, all_values, all_gates)
 
@@ -633,13 +649,19 @@
             return pl.ds(flipped(me, steps[0]), 1)
         return pl.ds(flipped(me // 2, steps[0] // 2) * 2, 2)
 
+    def chunk_of(step):
+        return [step in steps for steps in CHUNKS].index(True)
+
+    def fwd_recv_of(step, which, part):
+        return fwd_recv.at[step, part] if which == 1 else both_recv.at[chunk_of(step)]
+
     def forward(step, which, part):
         block = pieces.at[across if which == 2 else mine, flipped(me, step), :, columns(part)]
         return remote(
             block,
             block,
-            fwd_send.at[which, step, part],
-            fwd_recv.at[which, step, part],
+            fwd_send.at[0],
+            fwd_recv_of(step, which, part),
             me,
             across if which == 1 else twin,
         )
@@ -651,8 +673,8 @@
         return remote(
             block,
             block,
-            fwd_send.at[which, step, part],
-            fwd_recv.at[which, step, part],
+            fwd_send.at[0],
+            fwd_recv_of(step, which, part),
             me,
             twin,
         )
@@ -672,7 +694,7 @@
         return remote(
             partial.at[:, 1 - core, pair, :, narrow(part)],
             from_core.at[:, pair, :, narrow(part)],
-            core_send.at[chunk, part],
+            core_send.at[0],
             core_recv.at[chunk, part],
             me,
             twin,
@@ -683,17 +705,15 @@
         return remote(
             to_chip.at[source, :, narrow(part)],
             from_chip.at[source, :, narrow(part)],
-            chip_send.at[step, part],
+            chip_send.at[0],
             chip_recv.at[step, part],
             me,
             across,
         )
 
     def stage_compute(chunk, _):
-        for step in CHUNKS[chunk]:
-            for part in range(HALVES):
-                forwarded(step, 0, part).wait_recv()
-                forwarded(step, 2, part).wait_recv()
+        landed = pieces.at[pl.ds(0, 2), pl.ds(0, len(CHUNKS[chunk]))]
+        pltpu.make_async_copy(landed, landed, both_recv.at[chunk]).wait()
         pair = pair_of(chunk)
         blocks = len(CHUNKS[chunk])
         count = GROUP * blocks * capacity
@@ -733,21 +753,18 @@
     def return_copy(peer, part):
         return remote(
             final.at[peer, :, narrow(part)],
-            returned.at[me, :, narrow(part)],
-            ret_send.at[peer, part],
-            ret_recv.at[me, part],
+            returned_out.at[me, :, narrow(part)],
+            ret_send.at[0],
+            ret_recv.at[0],
             peer,
             mine,
         )
 
-    def return_arrival(peer, part):
-        return remote(
-            final.at[peer, :, narrow(part)],
-            returned.at[peer, :, narrow(part)],
-            ret_send.at[peer, part],
-            ret_recv.at[peer, part],
-            peer,
-            mine,
+    def own_copy(part):
+        return pltpu.make_async_copy(
+            final.at[me, :, narrow(part)],
+            returned_out.at[me, :, narrow(part)],
+            output_sem.at[1 + part],
         )
 
     def stage_final(step, part):
@@ -759,18 +776,15 @@
             + from_core[side, source, :, span].astype(f32)
             + from_chip[source, :, span].astype(f32)
         ).astype(bf16)
+        final[source, :, span] = total
         if step:
-            final[source, :, span] = total
             return_copy(source, part).start()
         else:
-            returned[me, :, span] = total
-
-    result_copies = [
-        pltpu.make_async_copy(attended, attended_out, output_sem.at[0]),
-        pltpu.make_async_copy(expert_out, expert_result, output_sem.at[1]),
-    ]
-
-    def attend():
+            own_copy(part).start()
+
+    attended_copy = pltpu.make_async_copy(attended, attended_out, output_sem.at[0])
+
+    def attend(*_):
         wait_keys(1)
         length = n * rows
         every_key = all_keys[...].reshape(length, HEAD_WIDTH)
@@ -796,7 +810,7 @@
             total = jnp.sum(weights, axis=1, keepdims=True)
             mixed = jnp.dot(weights.astype(bf16), every_value, preferred_element_type=f32)
             attended[:, span] = (mixed / total).astype(bf16)
-        result_copies[0].start()
+        attended_copy.start()
 
     def keys_on(bit, _):
         wait_keys(bit)
@@ -806,9 +820,24 @@
         for copy in weight_copies:
             copy.wait()
 
+    def drain(*_):
+        for held, semaphore in (
+            (send.at[pl.ds(1, n - 1)], disp_send),
+            (pieces.at[pl.ds(0, 3)], fwd_send),
+            (from_core, core_send),
+        ):
+            pltpu.make_async_copy(held, held, semaphore.at[0]).wait()
+        for bit in bits:
+            for others in key_flips(bit):
+
+                @pl.when(sends_keys(bit, others))
+                def _():
+                    for which in range(3):
+                        key_send_copy(which, bit, others).wait_send()
+
     stages = (
         stage_arrive, stage_cross, stage_compute, stage_core_sum, stage_chip, stage_final,
-        keys_on, weights_in,
+        keys_on, weights_in, attend, drain,
     )
 
     def run(actions):
@@ -821,57 +850,54 @@
             run(actions)
         else:
             pl.when(inner == who)(functools.partial(run, tuple(actions)))
-    attend()
-
-    for step in range(1, n):
-        for part in range(HALVES):
-            return_arrival(flipped(me, step), part).wait_recv()
-    slot_iota = lax.broadcasted_iota(jnp.int32, (rows, slots), 1).astype(f32)
-    take = (slot_iota == slot).astype(f32).astype(bf16)
-    expert_out[...] = jnp.dot(
-        take, returned[...].reshape(slots, width), preferred_element_type=f32
-    ).astype(bf16)
-    result_copies[1].start()
-
-    for step in range(1, n):
-        peer = flipped(me, step)
-        for part in range(HALVES):
-            dispatch(peer, part).wait_send()
-            return_copy(peer, part).wait_send()
+    for held, semaphore in (
+        (final.at[pl.ds(1, n - 1)], ret_recv),
+        (to_chip, chip_send),
+        (final.at[pl.ds(1, n - 1)], ret_send),
+    ):
+        pltpu.make_async_copy(held, held, semaphore.at[0]).wait()
+    attended_copy.wait()
     for part in range(HALVES):
-        for chunk in range(len(CHUNKS)):
-            core_copy(chunk, part).wait_send()
-        for step in range(n):
-            for which in range(3):
-                forward(step, which, part).wait_send()
-            chip_copy(step, part).wait_send()
-    for bit in bits:
-        for others in key_flips(bit):
-
-            @pl.when(sends_keys(bit, others))
-            def _():
-                for which in range(3):
-                    key_send_copy(which, bit, others).wait_send()
-    for copy in result_copies:
-        copy.wait()
-
-
-def handed_on(first, second, first_out, second_out, first_held, second_held, taken, given):
-    arrays = ((first, first_held, first_out), (second, second_held, second_out))
+        own_copy(part).wait()
+
+
+def gather_kernel(
+    capacity, attended_in, returned_in, route_in, attended_out, expert_result, attended, returned,
+    route_group, expert_out, taken, given,
+):
+    f32, bf16 = jnp.float32, jnp.bfloat16
+    slots, width = returned.shape
+    rows = expert_out.shape[0]
+    tile = math.gcd(width, 1024)
+    spans = [pl.ds(start, tile) for start in range(0, width, tile)]
+    route = pltpu.make_async_copy(route_in, route_group, taken.at[0])
     takes = [
-        pltpu.make_async_copy(source, held, taken.at[index])
-        for index, (source, held, _) in enumerate(arrays)
+        pltpu.make_async_copy(returned_in.at[:, span], returned.at[:, span], taken.at[2 + index])
+        for index, span in enumerate(spans)
     ]
     gives = [
-        pltpu.make_async_copy(held, target, given.at[index])
-        for index, (_, held, target) in enumerate(arrays)
+        pltpu.make_async_copy(
+            expert_out.at[:, span], expert_result.at[:, span], given.at[1 + index]
+        )
+        for index, span in enumerate(spans)
     ]
-    for copy in takes:
+    attended_take = pltpu.make_async_copy(attended_in, attended, taken.at[1])
+    attended_give = pltpu.make_async_copy(attended, attended_out, given.at[0])
+    for copy in (route, *takes, attended_take):
         copy.start()
-    for take, give in zip(takes, gives):
+    route.wait()
+    slot = slots_of(route_group, capacity)
+    slot_iota = lax.broadcasted_iota(jnp.int32, (rows, slots), 1).astype(f32)
+    choose = (slot_iota == slot).astype(f32).astype(bf16)
+    for span, take, give in zip(spans, takes, gives):
         take.wait()
+        expert_out[:, span] = jnp.dot(
+            choose, returned[:, span], preferred_element_type=f32
+        ).astype(bf16)
         give.start()
-    for copy in gives:
+    attended_take.wait()
+    attended_give.start()
+    for copy in (*gives, attended_give):
         copy.wait()
 
 
@@ -892,20 +918,19 @@
         queries, keys, values, cum_gates.T, expert_in, norm_gain.reshape(1, width), route_group.T,
         route_member.T, route_weight.T,
     )
-    results = pl.pallas_call(
+    attended, returned = pl.pallas_call(
         functools.partial(fused_kernel, n, capacity),
         out_shape=(
             jax.ShapeDtypeStruct(queries.shape, bf16),
-            jax.ShapeDtypeStruct(expert_in.shape, bf16),
+            jax.ShapeDtypeStruct(block, bf16),
         ),
         in_specs=[anywhere] * 12,
         out_specs=(anywhere, anywhere),
         scratch_shapes=[
             *(pltpu.VMEM(array.shape, array.dtype) for array in inputs),
             pltpu.VMEM(queries.shape, bf16),
-            pltpu.VMEM(expert_in.shape, bf16),
             dma((len(inputs),)),
-            dma((2,)),
+            dma((1 + HALVES,)),
             pltpu.VMEM((n, capacity, wide), bf16),
             pltpu.VMEM((GROUP, n, capacity, wide), bf16),
             pltpu.VMEM((width, 2 * hidden_width), bf16),
@@ -915,22 +940,22 @@
             pltpu.VMEM(block, bf16),
             pltpu.VMEM(block, bf16),
             pltpu.VMEM(block, bf16),
-            pltpu.VMEM(block, bf16),
             pltpu.VMEM((n,) + keys.shape, bf16),
             pltpu.VMEM((n,) + values.shape, bf16),
             pltpu.VMEM((8, rows), jnp.float32),
             pltpu.VMEM((n, 8, rows), jnp.float32),
             dma((3,)),
+            dma((1,)),
             dma((n, HALVES)),
+            dma((1,)),
             dma((n, HALVES)),
-            dma((3, n, HALVES)),
-            dma((3, n, HALVES)),
+            dma((len(CHUNKS),)),
+            dma((1,)),
             dma((len(CHUNKS), HALVES)),
-            dma((len(CHUNKS), HALVES)),
+            dma((1,)),
             dma((n, HALVES)),
-            dma((n, HALVES)),
-            dma((n, HALVES)),
-            dma((n, HALVES)),
+            dma((1,)),
+            dma((1,)),
             dma((3, n)),
             dma((3, n)),
         ],
@@ -941,18 +966,26 @@
     )(
         *inputs, w_gate, w_up, w_down,
     )
+    slots = n * capacity
+    tiles = width // math.gcd(width, 1024)
     return pl.pallas_call(
-        handed_on,
-        out_shape=tuple(jax.ShapeDtypeStruct(result.shape, bf16) for result in results),
-        in_specs=[anywhere, anywhere],
+        functools.partial(gather_kernel, capacity),
+        out_shape=(
+            jax.ShapeDtypeStruct(queries.shape, bf16),
+            jax.ShapeDtypeStruct(expert_in.shape, bf16),
+        ),
+        in_specs=[anywhere] * 3,
         out_specs=(anywhere, anywhere),
         scratch_shapes=[
-            *(pltpu.VMEM(result.shape, bf16) for result in results),
-            dma((2,)),
-            dma((2,)),
+            pltpu.VMEM(queries.shape, bf16),
+            pltpu.VMEM((slots, width), bf16),
+            pltpu.VMEM((1, rows), jnp.int32),
+            pltpu.VMEM(expert_in.shape, bf16),
+            dma((2 + tiles,)),
+            dma((1 + tiles,)),
         ],
-        name="handed_on",
-    )(*results)
+        name="gathered",
+    )(attended, returned.reshape(slots, width), route_group.T)
 
 
 def per_device(

time: 89.3 us -> 85.9 us (0.962)
  Pallas kernels: 88.3 us -> 85 us
    pallas_call x1, Pallas kernels: 86 us -> 82.2 us  [fused(): pl.pallas_call(functools.partial(fused_kernel, n, capacity), out_shape=(j...]
where the time goes in v2:
time: 85.9 us; the launch traced here: 85.8 us
  Pallas kernels  85 us (99%)
    pallas_call x1, Pallas kernels, fused(): pl.pallas_call(functools.partial(fused_kernel, n, capacity), out_shape=(j...  82.2 us
    pallas_call x1, Pallas kernels, fused(): pl.pallas_call(functools.partial(gather_kernel, capacity), out_shape=(jax...  2.77 us

profile of v2, /device:TPU:0, one launch (start us, length us, event | category | flops | bytes accessed | tf_op | source)
XLA Modules:
  0.0 85.8 jit_solution(2037754026828280362)
XLA Ops:
  0.6 82.2 %fused.1 = (bf16[128,512]{1,0:T(8,128)(2,1)}, bf16[8,24,4096]{2,1,0:T(8,128)(2,1)}) custom-call(bf16[128,512]{1,0:T(8,128)(2,1)} %queries_in.1, bf16[128,128]{1,0:T(8,128)(2,1)} %keys_in.1, bf16[128,128]{1,0:T(8,128)(2,1)} %values_in.1, f32[4,128]{1,0:T(4,128)} %bitcast.10, bf16[128,4096]{1,0:T(8,128)(2,1)} %expert_rows.1, f32[1,4096]{1,0:T(1,128)} %bitcast.7, ...), custom_call_target="tpu_custom_call" | custom-call | tf_op jit(solution)/shard_map/fused/pallas_call | solution.py:921
  82.8 2.8 %gathered.1 = (bf16[128,512]{1,0:T(8,128)(2,1)}, bf16[128,4096]{1,0:T(8,128)(2,1)}) custom-call(bf16[128,512]{1,0:T(8,128)(2,1)} %get-tuple-element.4.attended_in, bf16[192,4096]{1,0:T(8,128)(2,1)} %bitcast.6, s32[1,128]{1,0:T(1,128)} %bitcast.9), custom_call_target="tpu_custom_call" | custom-call | tf_op jit(solution)/shard_map/gathered/pallas_call | solution.py:971

commit v3 on v2

--- a/solution.py
+++ b/solution.py
@@ -131,7 +131,7 @@
     (OUTER, KEYS, 2, 0),
     (BOTH, FINAL, 3, 1),
     (OUTER, FINAL, 4, 0),
-    (OUTER, CHIP, 1, 1),
+    (OUTER, CHIP, 3, 0),
     (INNER, CHIP, 2, 0),
     (INNER, CORE_SUM, 1, 1),
     (INNER, CHIP, 2, 1),
@@ -147,15 +147,15 @@
     (INNER, FINAL, 6, 1),
     (INNER, FINAL, 2, 0),
     (BOTH, FINAL, 1, 0),
-    (OUTER, CHIP, 3, 0),
+    (OUTER, CHIP, 1, 1),
     (OUTER, CHIP, 0, 1),
     (INNER, ATTEND, 0, 0),
     (INNER, FINAL, 6, 0),
     (BOTH, FINAL, 2, 1),
     (OUTER, CHIP, 0, 0),
     (OUTER, FINAL, 2, 0),
+    (OUTER, FINAL, 3, 0),
     (OUTER, ATTEND, 0, 0),
-    (OUTER, FINAL, 3, 0),
     (OUTER, FINAL, 1, 1),
     (INNER, CHIP, 0, 1),
     (BOTH, DRAIN, 0, 0),
@@ -413,8 +413,7 @@
     to_chip,
     from_chip,
     final,
-    all_keys,
-    all_values,
+    all_pairs,
     own_gates,
     all_gates,
     weight_sem,
@@ -586,16 +585,15 @@
         @pl.when(jnp.logical_not(has(me, 1 << (flip.bit_length() - 1))))
         def _():
             block = flipped(me, flip)
-            all_keys[block] = jnp.zeros_like(all_keys[block])
-            all_values[block] = jnp.zeros_like(all_values[block])
+            all_pairs[block] = jnp.zeros_like(all_pairs[block])
             all_gates[block] = jnp.zeros_like(all_gates[block])
 
     all_gates[me] = own_gates[...]
-    all_keys[me] = keys[...]
-    all_values[me] = values[...]
-
-
-    shared = (all_keys, all_values, all_gates)
+    all_pairs[me, pl.ds(0, rows), :] = keys[...]
+    all_pairs[me, pl.ds(rows, rows), :] = values[...]
+
+
+    shared = (all_pairs, all_gates)
 
     bits = [1 << power for power in reversed(range((n - 1).bit_length()))]
 
@@ -632,7 +630,7 @@
 
             @pl.when(has(me, high(flip)))
             def _():
-                for which in range(3):
+                for which in range(2):
                     key_arrival(which, flip).wait_recv()
 
     def start_keys(bit):
@@ -640,7 +638,7 @@
 
             @pl.when(sends_keys(bit, others))
             def _():
-                for which in range(3):
+                for which in range(2):
                     key_send_copy(which, bit, others).start()
 
     def pair_of(chunk):
@@ -787,8 +785,8 @@
     def attend(*_):
         wait_keys(1)
         length = n * rows
-        every_key = all_keys[...].reshape(length, HEAD_WIDTH)
-        every_value = all_values[...].reshape(length, HEAD_WIDTH)
+        every_key = all_pairs[:, pl.ds(0, rows), :].reshape(length, HEAD_WIDTH)
+        every_value = all_pairs[:, pl.ds(rows, rows), :].reshape(length, HEAD_WIDTH)
         key_pos = lax.broadcasted_iota(jnp.int32, (rows, length), 1)
         query_pos = lax.broadcasted_iota(jnp.int32, (rows, length), 0) + me * rows
         allowed = key_pos <= query_pos
@@ -832,7 +830,7 @@
 
                 @pl.when(sends_keys(bit, others))
                 def _():
-                    for which in range(3):
+                    for which in range(2):
                         key_send_copy(which, bit, others).wait_send()
 
     stages = (
@@ -940,8 +938,7 @@
             pltpu.VMEM(block, bf16),
             pltpu.VMEM(block, bf16),
             pltpu.VMEM(block, bf16),
-            pltpu.VMEM((n,) + keys.shape, bf16),
-            pltpu.VMEM((n,) + values.shape, bf16),
+            pltpu.VMEM((n, 2 * rows, keys.shape[1]), bf16),
             pltpu.VMEM((8, rows), jnp.float32),
             pltpu.VMEM((n, 8, rows), jnp.float32),
             dma((3,)),
@@ -956,8 +953,8 @@
             dma((n, HALVES)),
             dma((1,)),
             dma((1,)),
-            dma((3, n)),
-            dma((3, n)),
+            dma((2, n)),
+            dma((2, n)),
         ],
         compiler_params=pltpu.CompilerParams(
             collective_id=0, has_side_effects=True, vmem_limit_bytes=62 * 1024 * 1024

time: 85.9 us -> 85.8 us (level)
  no operation moved by 1% of the time
where the time goes in v3:
time: 85.8 us; the launch traced here: 85.6 us
  Pallas kernels  84.8 us (99%)
    pallas_call x1, Pallas kernels, fused(): pl.pallas_call(functools.partial(fused_kernel, n, capacity), out_shape=(j...  82.1 us
    pallas_call x1, Pallas kernels, fused(): pl.pallas_call(functools.partial(gather_kernel, capacity), out_shape=(jax...  2.77 us

profile of v3, /device:TPU:0, one launch (start us, length us, event | category | flops | bytes accessed | tf_op | source)
XLA Modules:
  0.0 85.6 jit_solution(842656724071458626)
XLA Ops:
  0.6 82.1 %fused.1 = (bf16[128,512]{1,0:T(8,128)(2,1)}, bf16[8,24,4096]{2,1,0:T(8,128)(2,1)}) custom-call(bf16[128,512]{1,0:T(8,128)(2,1)} %queries_in.1, bf16[128,128]{1,0:T(8,128)(2,1)} %keys_in.1, bf16[128,128]{1,0:T(8,128)(2,1)} %values_in.1, f32[4,128]{1,0:T(4,128)} %bitcast.10, bf16[128,4096]{1,0:T(8,128)(2,1)} %expert_rows.1, f32[1,4096]{1,0:T(1,128)} %bitcast.7, ...), custom_call_target="tpu_custom_call" | custom-call | tf_op jit(solution)/shard_map/fused/pallas_call | solution.py:919
  82.7 2.8 %gathered.1 = (bf16[128,512]{1,0:T(8,128)(2,1)}, bf16[128,4096]{1,0:T(8,128)(2,1)}) custom-call(bf16[128,512]{1,0:T(8,128)(2,1)} %get-tuple-element.4.attended_in, bf16[192,4096]{1,0:T(8,128)(2,1)} %bitcast.6, s32[1,128]{1,0:T(1,128)} %bitcast.9), custom_call_target="tpu_custom_call" | custom-call | tf_op jit(solution)/shard_map/gathered/pallas_call | solution.py:968
